TPU v7x, 32 devices: a whole 2x2x4 slice. The times are simulated.
32 devices in a mesh: ra: 8 (over z, y), cb: 4 (over x, core).
Axes of the slice: x: 2, y: 2, z: 4, core: 2. Of those that a mesh axis runs over, the one named last changes fastest.
Arguments:
- tokens: bfloat16 [4, 128, 4096], P(None, None, 'ra'), may hold values from -64 to 64
- norm_gain: float32 [2, 4096], P(None, 'ra'), may hold values from 0.1 to 1.9
- gate_weight: bfloat16 [2, 4096, 11264], P(None, 'ra', 'cb'), may hold values from -0.09375 to 0.09375
- up_weight: bfloat16 [2, 4096, 11264], P(None, 'ra', 'cb'), may hold values from -0.09375 to 0.09375
- gate_taps: float32 [2, 3, 11264], P(None, None, 'cb'), may hold values from -3 to 3
- up_taps: float32 [2, 3, 11264], P(None, None, 'cb'), may hold values from -3 to 3
- gate_bias: float32 [2, 11264], P(None, 'cb'), may hold values from -3 to 3
- up_bias: float32 [2, 11264], P(None, 'cb'), may hold values from -3 to 3
- down_weight: bfloat16 [2, 11264, 4096], P(None, 'cb', 'ra'), may hold values from -0.0546875 to 0.0546875
Outputs:
- mixed: bfloat16 [4, 128, 4096], P(None, None, 'ra')
All inputs are finite; a program needn't handle non-finite values.
Results may differ from a plain program's by a relative error of at most 0.03.
Values may be sent and summed in bfloat16 or wider, within the bound.
A program may use at most 64 MiB of HBM per device.

v0:
```python
import jax
import jax.numpy as jnp
from jax import lax
from jax.sharding import PartitionSpec as P

D = 4096
KERNEL = 3
LAYERS = 2
eps = 1e-06
resid_scale = 0.5


def causal_conv(projected, kernel, offsets, seqs, length):
    values = projected.astype(jnp.float32).reshape(seqs, length, 2, projected.shape[2])
    padded = jnp.pad(values, ((0, 0), (KERNEL - 1, 0), (0, 0), (0, 0)))
    result = offsets
    for tap_idx in range(KERNEL):
        result = result + kernel[tap_idx] * padded[:, tap_idx : tap_idx + length]
    return result.reshape(seqs * length, 2, projected.shape[2])


def per_device(
    tokens, norm_gain, gate_weight, up_weight, gate_taps, up_taps, gate_bias, up_bias, down_weight
):
    seqs, length, width_local = tokens.shape
    rows_count = seqs * length
    carried = tokens.reshape(rows_count, width_local).astype(jnp.float32)
    for layer_idx in range(LAYERS):
        local_squares = jnp.sum(carried * carried, axis=1)
        scaled = (carried * norm_gain[layer_idx]).astype(jnp.bfloat16)
        kernel = jnp.stack([gate_taps[layer_idx], up_taps[layer_idx]], axis=1)
        offsets = jnp.stack([gate_bias[layer_idx], up_bias[layer_idx]], axis=0)
        down_local = down_weight[layer_idx]
        partial_value = jnp.stack(
            [
                jnp.dot(scaled, gate_weight[layer_idx], preferred_element_type=jnp.float32),
                jnp.dot(scaled, up_weight[layer_idx], preferred_element_type=jnp.float32),
            ],
            axis=1,
        )
        row_squares = lax.psum(local_squares, "ra")
        summed = lax.psum(partial_value.astype(jnp.bfloat16), "ra").astype(jnp.float32)
        inverse = lax.rsqrt(row_squares / D + eps)
        projected = (summed * inverse[:, None, None]).astype(jnp.bfloat16)
        convolved = causal_conv(projected, kernel, offsets, seqs, length)
        hidden = (jax.nn.silu(convolved[:, 0]) * convolved[:, 1]).astype(jnp.bfloat16)
        branch_part = jnp.dot(hidden, down_local, preferred_element_type=jnp.float32)
        branch = lax.psum(branch_part.astype(jnp.bfloat16), "cb").astype(jnp.float32)
        carried = resid_scale * carried + branch
    return carried.astype(jnp.bfloat16).reshape(seqs, length, width_local)


def solution(mesh):
    in_specs = (
        P(None, None, "ra"),
        P(None, "ra"),
        P(None, "ra", "cb"),
        P(None, "ra", "cb"),
        P(None, None, "cb"),
        P(None, None, "cb"),
        P(None, "cb"),
        P(None, "cb"),
        P(None, "cb", "ra"),
    )
    out_specs = P(None, None, "ra")
    return jax.shard_map(
        per_device, mesh=mesh, in_specs=in_specs, out_specs=out_specs, check_vma=False
    )
```

profile of v0, /device:TPU:0, one launch (start us, length us, event | category | flops | bytes accessed | tf_op | source)
XLA Modules:
  0.0 539.4 jit_solution(4109739938134989243)
XLA Ops:
  6.5 0.0 all-reduce.7.cloned.1.call-start
  6.5 0.9 fusion.60
  7.4 1.5 convert_multiply_fusion.2
  8.9 3.5 fusion.13
  12.3 0.0 copy-done.5
  12.4 1.7 fusion.12
  14.0 3.0 pad_maximum_fusion
  17.1 0.0 all-reduce.7.cloned.1.call-update
  17.1 0.0 all-reduce.9.cloned.1.call-start
  17.1 24.1 %psum.43 = f32[512]{0:T(512)S(1)} all-reduce(f32[512]{0:T(512)S(1)} %bitcast.89), channel_id=1, replica_groups=mesh['ra'=8,'cb'=4] {'ra'}, use_global_device_ids=true, to_apply=%region_2.0 | all-reduce | flops 512 | bytes 4096 | tf_op jit(solution)/shard_map/psum | solution.py:41
  41.2 0.0 copy-done.3
  41.3 0.0 copy-done.4
  41.4 0.0 copy-done.1
  41.4 0.0 copy-done.2
  41.4 0.1 slice_bitcast_fusion
  41.5 0.1 fusion.52
  41.6 177.0 %all-reduce.7.cloned.1.call-done = bf16[512,2,2816]{2,0,1:T(8,128)(2,1)} async-done(((bf16[512,2,2816]{2,0,1:T(8,128)(2,1)}), bf16[512,2,2816]{2,0,1:T(8,128)(2,1)}) %all-reduce.7.cloned.1.call-update) | async-done | bytes 5767184 | tf_op jit(solution)/shard_map/psum | solution.py:42
  218.5 4.2 multiply_convert_fusion.1
  222.7 0.0 slice-start
  222.8 1.0 convert.22
  223.8 0.0 slice-start.1
  223.8 6.3 %fusion.3 = f32[4,128,2,2816]{3,1,0,2:T(8,128)} fusion(f32[4,128,2,2816]{3,1,0,2:T(8,128)S(1)} %convert.22, f32[2,2816]{1,0:T(2,128)S(1)} %get-tuple-element.18, f32[2,2816]{1,0:T(2,128)S(1)} %get-tuple-element.19, f32[2,2816]{1,0:T(2,128)S(1)} %get-tuple-element.17, f32[2,2816]{1,0:T(2,128)S(1)} %get-tuple-element.28), kind=kLoop, calls=%fused_computation.7 | loop fusion | flops 17301504 | bytes 23158784 | tf_op jit(solution)/shard_map/add | solution.py:18
  230.1 0.0 slice-done
  230.1 0.0 slice-done.1
  230.1 6.9 %fusion.34 = bf16[512,512]{1,0:T(8,128)(2,1)} fusion(bf16[2,2816,512]{2,1,0:T(8,128)(2,1)S(1)} %bitcast.93, f32[512,2,2816]{2,0,1:T(8,128)} %bitcast.85), kind=kOutput, calls=%fused_computation.49 | convolution fusion | flops 1485307904 | bytes 14942208 | tf_op jit(solution)/shard_map/dot_general | solution.py:47
  237.0 0.0 all-reduce.9.cloned.1.call-update
  237.0 0.2 all-reduce.11.cloned.1.call-start
  237.3 32.3 %all-reduce.9.cloned.1.call-done = bf16[512,512]{1,0:T(8,128)(2,1)} async-done(((bf16[512,512]{1,0:T(8,128)(2,1)}), bf16[512,512]{1,0:T(8,128)(2,1)}) %all-reduce.9.cloned.1.call-update) | async-done | bytes 524304 | tf_op jit(solution)/shard_map/psum | solution.py:48
  269.6 1.3 multiply_reduce_fusion
  270.9 3.5 fusion.15
  274.4 3.5 fusion.14
  277.9 3.0 pad_maximum_fusion.1
  280.9 0.0 all-reduce.11.cloned.1.call-update
  280.9 0.0 all-reduce.13.cloned.1.call-start
  281.0 0.1 fusion.54
  281.0 22.5 %psum.46 = f32[512]{0:T(512)S(1)} all-reduce(f32[512]{0:T(512)S(1)} %get-tuple-element.5), channel_id=1, replica_groups=mesh['ra'=8,'cb'=4] {'ra'}, use_global_device_ids=true, to_apply=%region_6.7 | all-reduce | flops 512 | bytes 4096 | tf_op jit(solution)/shard_map/psum | solution.py:41
  303.5 176.2 %all-reduce.11.cloned.1.call-done = bf16[512,2,2816]{2,0,1:T(8,128)(2,1)} async-done(((bf16[512,2,2816]{2,0,1:T(8,128)(2,1)}), bf16[512,2,2816]{2,0,1:T(8,128)(2,1)}) %all-reduce.11.cloned.1.call-update) | async-done | bytes 5767184 | tf_op jit(solution)/shard_map/psum | solution.py:42
  479.7 4.2 multiply_convert_fusion
  483.9 0.0 slice-start.2
  483.9 1.0 convert.23
  484.9 0.0 slice-start.3
  485.0 6.3 %fusion.8 = f32[4,128,2,2816]{3,1,0,2:T(8,128)} fusion(f32[4,128,2,2816]{3,1,0,2:T(8,128)S(1)} %convert.23, f32[2,2816]{1,0:T(2,128)S(1)} %get-tuple-element.11, f32[2,2816]{1,0:T(2,128)S(1)} %get-tuple-element.12, f32[2,2816]{1,0:T(2,128)S(1)} %get-tuple-element.10, f32[2,2816]{1,0:T(2,128)S(1)} %get-tuple-element.29), kind=kLoop, calls=%fused_computation.12 | loop fusion | flops 17301504 | bytes 23158784 | tf_op jit(solution)/shard_map/add | solution.py:18
  491.2 0.0 slice-done.2
  491.2 0.0 slice-done.3
  491.2 7.0 %fusion.39 = bf16[512,512]{1,0:T(8,128)(2,1)} fusion(bf16[2,2816,512]{2,1,0:T(8,128)(2,1)S(1)} %bitcast.95, f32[512,2,2816]{2,0,1:T(8,128)} %bitcast.86), kind=kOutput, calls=%fused_computation.50 | convolution fusion | flops 1485307904 | bytes 14942208 | tf_op jit(solution)/shard_map/dot_general | solution.py:47
  498.2 0.0 all-reduce.13.cloned.1.call-update
  498.3 32.5 %all-reduce.13.cloned.1.call-done = bf16[512,512]{1,0:T(8,128)(2,1)} async-done(((bf16[512,512]{1,0:T(8,128)(2,1)}), bf16[512,512]{1,0:T(8,128)(2,1)}) %all-reduce.13.cloned.1.call-update) | async-done | bytes 524304 | tf_op jit(solution)/shard_map/psum | solution.py:48
  530.8 2.0 add_convert_fusion
  (14 shorter events, 0.1 us)
Async XLA Ops:
  6.5 212.0 %all-reduce.7.cloned.1.call-start = ((), (), s32[]{:S(2)}) async-start(), calls=%async_computation | async-start | bytes 11534336 | tf_op jit(solution)/shard_map/psum | solution.py:42
  6.5 5.8 %copy-start.5 = (bf16[2,512,2816]{2,1,0:T(8,128)(2,1)S(1)}, bf16[2,512,2816]{2,1,0:T(8,128)(2,1)}, u32[]{:S(2)}) copy-start(bf16[2,512,2816]{2,1,0:T(8,128)(2,1)} %param.11) | copy-start | bytes 17301508
  17.1 24.2 %copy-start.3 = (f32[2,2816]{1,0:T(2,128)S(1)}, f32[2,2816]{1,0:T(2,128)}, u32[]{:S(2)}) copy-start(f32[2,2816]{1,0:T(2,128)} %param.15) | copy-start | bytes 67588
  17.1 24.2 %copy-start.4 = (f32[2,2816]{1,0:T(2,128)S(1)}, f32[2,2816]{1,0:T(2,128)}, u32[]{:S(2)}) copy-start(f32[2,2816]{1,0:T(2,128)} %param.16) | copy-start | bytes 67588
  17.1 24.3 %copy-start.1 = (f32[2,3,2816]{2,0,1:T(2,128)S(1)}, f32[2,3,2816]{2,0,1:T(2,128)}, u32[]{:S(2)}) copy-start(f32[2,3,2816]{2,0,1:T(2,128)} %param.14) | copy-start | bytes 202756
  17.1 24.3 %copy-start.2 = (f32[2,3,2816]{2,0,1:T(2,128)S(1)}, f32[2,3,2816]{2,0,1:T(2,128)}, u32[]{:S(2)}) copy-start(f32[2,3,2816]{2,0,1:T(2,128)} %param.13) | copy-start | bytes 202756
  17.1 252.5 %all-reduce.9.cloned.1.call-start = ((), (), s32[]{:S(2)}) async-start(), calls=%async_computation.1 | async-start | bytes 1048576 | tf_op jit(solution)/shard_map/psum | solution.py:48
  222.7 7.3 %slice-start = ((s8[5767168]{0:T(1024)(128)(4,1)}), s8[1572864]{0:T(1024)(128)(4,1)S(1)}, s32[]{:S(2)}) async-start(s8[5767168]{0:T(1024)(128)(4,1)} %bitcast.92), calls=%async_computation.4 | async-start | bytes 3145728
  223.8 6.3 %slice-start.1 = ((s8[5767168]{0:T(1024)(128)(4,1)}), s8[4194304]{0:T(1024)(128)(4,1)S(1)}, s32[]{:S(2)}) async-start(s8[5767168]{0:T(1024)(128)(4,1)} %bitcast.92), calls=%async_computation.5 | async-start | bytes 8388608
  237.0 242.6 %all-reduce.11.cloned.1.call-start = ((), (), s32[]{:S(2)}) async-start(), calls=%async_computation.2 | async-start | bytes 11534336 | tf_op jit(solution)/shard_map/psum | solution.py:42
  280.9 249.9 %all-reduce.13.cloned.1.call-start = ((), (), s32[]{:S(2)}) async-start(), calls=%async_computation.3 | async-start | bytes 1048576 | tf_op jit(solution)/shard_map/psum | solution.py:48
  483.9 7.3 %slice-start.2 = ((s8[5767168]{0:T(1024)(128)(4,1)}), s8[1572864]{0:T(1024)(128)(4,1)S(1)}, s32[]{:S(2)}) async-start(s8[5767168]{0:T(1024)(128)(4,1)} %bitcast.94), calls=%async_computation.6 | async-start | bytes 3145728
  484.9 6.3 %slice-start.3 = ((s8[5767168]{0:T(1024)(128)(4,1)}), s8[4194304]{0:T(1024)(128)(4,1)S(1)}, s32[]{:S(2)}) async-start(s8[5767168]{0:T(1024)(128)(4,1)} %bitcast.94), calls=%async_computation.7 | async-start | bytes 8388608
  491.2 39.5 %copy-start = (bf16[512,512]{1,0:T(8,128)(2,1)S(1)}, bf16[512,512]{1,0:T(8,128)(2,1)}, u32[]{:S(2)}) copy-start(bf16[512,512]{1,0:T(8,128)(2,1)} %all-reduce.9.cloned.1.call-done) | copy-start | bytes 1572868
Sparse Core Ops, SparseCore 0:
  17.2 201.2 all-reduce.6
  237.2 32.3 all-reduce.8
  281.0 198.6 all-reduce.10
  498.4 32.3 all-reduce.12
where the time goes:
time: 540 us; the launch traced here: 539 us
  waiting for transfers between devices  418 us (77%)
  blocking collectives  46.6 us (9%)
  other arithmetic  34.1 us (6%)
  matrix products  26 us (5%)
  between operations  13.3 us (2%)
    psum x2, waiting for transfers between devices, per_device(): lax.psum(partial_value.astype(jnp.bfloat16), 'ra').astype(jnp.float32)  353 us
    psum x2, waiting for transfers between devices, per_device(): lax.psum(branch_part.astype(jnp.bfloat16), 'cb').astype(jnp.float32)  64.8 us
    psum x2, blocking collectives, per_device(): row_squares = lax.psum(local_squares, 'ra')  46.6 us
    dot_general x2, matrix products, per_device(): jnp.dot(hidden, down_local, preferred_element_type=jnp.float32)  13.9 us
    add x2, other arithmetic, causal_conv(): result = result + kernel[tap_idx] * padded[:, tap_idx:tap_idx + length]  12.6 us
  transfers between devices with their start and end apart: 4, of which 4 were waited for; matrix products, arithmetic and copies ran while one was open for 0% of the time, Pallas kernels for 0%

commit v1 on v0

--- a/solution.py
+++ b/solution.py
@@ -38,7 +38,13 @@
             ],
             axis=1,
         )
-        row_squares = lax.psum(local_squares, "ra")
+        devices = lax.axis_size("ra")
+        row_squares, far = (local_squares, 1)
+        while far < devices:
+            row_squares = row_squares + lax.ppermute(
+                row_squares, "ra", [(i, i ^ far) for i in range(devices)]
+            )
+            far = 2 * far
         summed = lax.psum(partial_value.astype(jnp.bfloat16), "ra").astype(jnp.float32)
         inverse = lax.rsqrt(row_squares / D + eps)
         projected = (summed * inverse[:, None, None]).astype(jnp.bfloat16)

time: 540 us -> 539 us (level)
  blocking collectives: 46.6 us -> 0 us
  waiting for transfers between devices: 418 us -> 451 us
  starting transfers between devices: 0.31 us -> 13.9 us
    psum x2 -> x0, blocking collectives: 46.6 us -> none  [per_device(): row_squares = lax.psum(local_squares, 'ra')]
    psum x2, waiting for transfers between devices: 353 us -> 373 us  [per_device(): lax.psum(partial_value.astype(jnp.bfloat16), 'ra').astype(jnp.float32)]
    ppermute x0 -> x6, starting transfers between devices: none -> 13.6 us  [per_device(): lax.ppermute(row_squares, 'ra', [(i, i ^ far) for i in range(devices)])]
    ppermute x0 -> x6, waiting for transfers between devices: none -> 13 us  [per_device(): lax.ppermute(row_squares, 'ra', [(i, i ^ far) for i in range(devices)])]
  transfers between devices with their start and end apart: 4 -> 10, of which waited for: 4 -> 10; matrix products, arithmetic and copies ran while one was open for 0% -> 0% of each run, Pallas kernels for 0% -> 0%
where the time goes in v1:
time: 539 us
  waiting for transfers between devices  451 us (84%)
  other arithmetic  33.9 us (6%)
  matrix products  26 us (5%)
  starting transfers between devices  13.9 us (3%)
  between operations  13.3 us (2%)
    psum x2, waiting for transfers between devices, per_device(): lax.psum(partial_value.astype(jnp.bfloat16), 'ra').astype(jnp.float32)  373 us
    psum x2, waiting for transfers between devices, per_device(): lax.psum(branch_part.astype(jnp.bfloat16), 'cb').astype(jnp.float32)  64.8 us
    dot_general x2, matrix products, per_device(): jnp.dot(hidden, down_local, preferred_element_type=jnp.float32)  13.9 us
    ppermute x6, starting transfers between devices, per_device(): lax.ppermute(row_squares, 'ra', [(i, i ^ far) for i in range(devices)])  13.6 us
    ppermute x6, waiting for transfers between devices, per_device(): lax.ppermute(row_squares, 'ra', [(i, i ^ far) for i in range(devices)])  13 us
    add x2, other arithmetic, causal_conv(): result = result + kernel[tap_idx] * padded[:, tap_idx:tap_idx + length]  12.4 us
  transfers between devices with their start and end apart: 10, of which 10 were waited for; matrix products, arithmetic and copies ran while one was open for 0% of the time, Pallas kernels for 0%

profile of v1, /device:TPU:0, one launch (start us, length us, event | category | flops | bytes accessed | tf_op | source)
XLA Modules:
  0.0 538.8 jit_solution(3745252764109744123)
XLA Ops:
  6.5 0.9 fusion.60
  7.4 1.5 convert_multiply_fusion.2
  8.9 3.5 fusion.13
  12.4 1.7 fusion.12
  14.0 3.0 pad_maximum_fusion
  17.1 0.0 all-reduce.7.cloned.1.call-update
  17.1 0.0 all-reduce.9.cloned.1.call-start
  17.1 3.1 collective-permute-start
  20.2 0.1 slice_bitcast_fusion
  20.4 1.4 collective-permute-done
  21.8 2.1 collective-permute-start.1
  23.8 0.1 fusion.52
  23.9 1.5 collective-permute-done.1
  25.4 3.0 collective-permute-start.2
  28.5 3.4 collective-permute-done.2
  31.9 186.4 %all-reduce.7.cloned.1.call-done = bf16[512,2,2816]{2,0,1:T(8,128)(2,1)} async-done(((bf16[512,2,2816]{2,0,1:T(8,128)(2,1)}), bf16[512,2,2816]{2,0,1:T(8,128)(2,1)}) %all-reduce.7.cloned.1.call-update) | async-done | bytes 5767184 | tf_op jit(solution)/shard_map/psum | solution.py:48
  218.3 4.2 multiply_convert_fusion.1
  222.5 0.0 slice-start
  222.5 1.0 convert.22
  223.6 0.0 slice-start.1
  223.6 6.2 %fusion.3 = f32[4,128,2,2816]{3,1,0,2:T(8,128)} fusion(f32[4,128,2,2816]{3,1,0,2:T(8,128)S(1)} %convert.22, f32[2,2816]{1,0:T(2,128)S(1)} %get-tuple-element.18, f32[2,2816]{1,0:T(2,128)S(1)} %get-tuple-element.19, f32[2,2816]{1,0:T(2,128)S(1)} %get-tuple-element.17, f32[2,2816]{1,0:T(2,128)S(1)} %get-tuple-element.28), kind=kLoop, calls=%fused_computation.7 | loop fusion | flops 17301504 | bytes 23158784 | tf_op jit(solution)/shard_map/add | solution.py:18
  229.8 6.9 %fusion.34 = bf16[512,512]{1,0:T(8,128)(2,1)} fusion(bf16[2,2816,512]{2,1,0:T(8,128)(2,1)S(1)} %bitcast.94, f32[512,2,2816]{2,0,1:T(8,128)} %bitcast.86), kind=kOutput, calls=%fused_computation.49 | convolution fusion | flops 1485307904 | bytes 14942208 | tf_op jit(solution)/shard_map/dot_general | solution.py:53
  236.7 0.0 all-reduce.9.cloned.1.call-update
  236.7 0.2 all-reduce.11.cloned.1.call-start
  237.0 32.3 %all-reduce.9.cloned.1.call-done = bf16[512,512]{1,0:T(8,128)(2,1)} async-done(((bf16[512,512]{1,0:T(8,128)(2,1)}), bf16[512,512]{1,0:T(8,128)(2,1)}) %all-reduce.9.cloned.1.call-update) | async-done | bytes 524304 | tf_op jit(solution)/shard_map/psum | solution.py:54
  269.3 1.3 multiply_reduce_fusion
  270.6 3.5 fusion.15
  274.1 3.5 fusion.14
  277.6 3.0 pad_maximum_fusion.1
  280.6 0.0 all-reduce.11.cloned.1.call-update
  280.6 0.0 all-reduce.13.cloned.1.call-start
  280.7 1.5 collective-permute-start.3
  282.2 2.1 collective-permute-done.3
  284.3 1.5 collective-permute-start.4
  285.8 2.1 collective-permute-done.4
  287.9 2.4 collective-permute-start.5
  290.3 0.1 fusion.54
  290.4 2.5 collective-permute-done.5
  292.9 186.3 %all-reduce.11.cloned.1.call-done = bf16[512,2,2816]{2,0,1:T(8,128)(2,1)} async-done(((bf16[512,2,2816]{2,0,1:T(8,128)(2,1)}), bf16[512,2,2816]{2,0,1:T(8,128)(2,1)}) %all-reduce.11.cloned.1.call-update) | async-done | bytes 5767184 | tf_op jit(solution)/shard_map/psum | solution.py:48
  479.2 4.2 multiply_convert_fusion
  483.4 0.0 slice-start.2
  483.4 1.0 convert.23
  484.5 0.0 slice-start.3
  484.5 6.2 %fusion.8 = f32[4,128,2,2816]{3,1,0,2:T(8,128)} fusion(f32[4,128,2,2816]{3,1,0,2:T(8,128)S(1)} %convert.23, f32[2,2816]{1,0:T(2,128)S(1)} %get-tuple-element.11, f32[2,2816]{1,0:T(2,128)S(1)} %get-tuple-element.12, f32[2,2816]{1,0:T(2,128)S(1)} %get-tuple-element.10, f32[2,2816]{1,0:T(2,128)S(1)} %get-tuple-element.29), kind=kLoop, calls=%fused_computation.12 | loop fusion | flops 17301504 | bytes 23158784 | tf_op jit(solution)/shard_map/add | solution.py:18
  490.7 7.0 %fusion.39 = bf16[512,512]{1,0:T(8,128)(2,1)} fusion(bf16[2,2816,512]{2,1,0:T(8,128)(2,1)S(1)} %bitcast.96, f32[512,2,2816]{2,0,1:T(8,128)} %bitcast.87), kind=kOutput, calls=%fused_computation.50 | convolution fusion | flops 1485307904 | bytes 14942208 | tf_op jit(solution)/shard_map/dot_general | solution.py:53
  497.7 0.0 all-reduce.13.cloned.1.call-update
  497.7 32.5 %all-reduce.13.cloned.1.call-done = bf16[512,512]{1,0:T(8,128)(2,1)} async-done(((bf16[512,512]{1,0:T(8,128)(2,1)}), bf16[512,512]{1,0:T(8,128)(2,1)}) %all-reduce.13.cloned.1.call-update) | async-done | bytes 524304 | tf_op jit(solution)/shard_map/psum | solution.py:54
  530.2 2.0 add_convert_fusion
  (28 shorter events, 0.1 us)
Async XLA Ops:
  6.5 211.8 %all-reduce.7.cloned.1.call-start = ((), (), s32[]{:S(2)}) async-start(), calls=%async_computation | async-start | bytes 11534336 | tf_op jit(solution)/shard_map/psum | solution.py:48
  6.5 5.8 %copy-start.5 = (bf16[2,512,2816]{2,1,0:T(8,128)(2,1)S(1)}, bf16[2,512,2816]{2,1,0:T(8,128)(2,1)}, u32[]{:S(2)}) copy-start(bf16[2,512,2816]{2,1,0:T(8,128)(2,1)} %param.11) | copy-start | bytes 17301508
  17.1 3.1 copy-start.3
  17.1 3.2 copy-start.1
  17.1 3.2 copy-start.2
  17.1 3.3 copy-start.4
  17.1 252.2 %all-reduce.9.cloned.1.call-start = ((), (), s32[]{:S(2)}) async-start(), calls=%async_computation.1 | async-start | bytes 1048576 | tf_op jit(solution)/shard_map/psum | solution.py:54
  17.1 4.6 collective-permute-start
  21.8 3.6 collective-permute-start.1
  25.4 6.5 %collective-permute-start.2 = (f32[512]{0:T(512)S(1)}, f32[512]{0:T(512)S(1)}, u32[]{:S(2)}, u32[]{:S(2)}) collective-permute-start(f32[512]{0:T(512)S(1)} %add.81), channel_id=1, source_target_pairs={{0,16},{4,20},{8,24},{12,28},{16,0},{20,4},{24,8},{28,12},{1,17},{... | collective-permute-start | bytes 6152 | tf_op jit(solution)/shard_map/ppermute | solution.py:44
  222.5 7.3 %slice-start = ((s8[5767168]{0:T(1024)(128)(4,1)}), s8[1572864]{0:T(1024)(128)(4,1)S(1)}, s32[]{:S(2)}) async-start(s8[5767168]{0:T(1024)(128)(4,1)} %bitcast.93), calls=%async_computation.4 | async-start | bytes 3145728
  223.6 6.2 %slice-start.1 = ((s8[5767168]{0:T(1024)(128)(4,1)}), s8[4194304]{0:T(1024)(128)(4,1)S(1)}, s32[]{:S(2)}) async-start(s8[5767168]{0:T(1024)(128)(4,1)} %bitcast.93), calls=%async_computation.5 | async-start | bytes 8388608
  236.7 242.5 %all-reduce.11.cloned.1.call-start = ((), (), s32[]{:S(2)}) async-start(), calls=%async_computation.2 | async-start | bytes 11534336 | tf_op jit(solution)/shard_map/psum | solution.py:48
  280.6 249.6 %all-reduce.13.cloned.1.call-start = ((), (), s32[]{:S(2)}) async-start(), calls=%async_computation.3 | async-start | bytes 1048576 | tf_op jit(solution)/shard_map/psum | solution.py:54
  280.7 3.7 collective-permute-start.3
  284.3 3.6 collective-permute-start.4
  287.9 5.0 collective-permute-start.5
  483.4 7.3 %slice-start.2 = ((s8[5767168]{0:T(1024)(128)(4,1)}), s8[1572864]{0:T(1024)(128)(4,1)S(1)}, s32[]{:S(2)}) async-start(s8[5767168]{0:T(1024)(128)(4,1)} %bitcast.95), calls=%async_computation.6 | async-start | bytes 3145728
  484.5 6.2 %slice-start.3 = ((s8[5767168]{0:T(1024)(128)(4,1)}), s8[4194304]{0:T(1024)(128)(4,1)S(1)}, s32[]{:S(2)}) async-start(s8[5767168]{0:T(1024)(128)(4,1)} %bitcast.95), calls=%async_computation.7 | async-start | bytes 8388608
  490.7 39.5 %copy-start = (bf16[512,512]{1,0:T(8,128)(2,1)S(1)}, bf16[512,512]{1,0:T(8,128)(2,1)}, u32[]{:S(2)}) copy-start(bf16[512,512]{1,0:T(8,128)(2,1)} %all-reduce.9.cloned.1.call-done) | copy-start | bytes 1572868
Sparse Core Ops, SparseCore 0:
  17.2 201.0 all-reduce.6
  236.9 32.3 all-reduce.8
  280.7 198.4 all-reduce.10
  497.8 32.3 all-reduce.12
